TPU v7x, 512 devices: a whole 4x4x16 slice. The times are simulated.
512 devices in a mesh: ep: 32 (over z, core), tp: 16 (over y, x).
Axes of the slice: x: 4, y: 4, z: 16, core: 2. Of those that a mesh axis runs over, the one named last changes fastest.
Arguments:
- mixer_rows: bfloat16 [8192, 2048], P('ep'), may hold values from -8 to 8
- mixer_gain: float32 [2048], replicated, may hold values from 0.1 to 1.9
- w_query: bfloat16 [2048, 1024], P(None, 'tp'), may hold values from -0.125 to 0.125
- w_key: bfloat16 [2048, 1024], P(None, 'tp'), may hold values from -0.125 to 0.125
- w_value: bfloat16 [2048, 1024], P(None, 'tp'), may hold values from -0.125 to 0.125
- key_shift: float32 [16, 8192], P('tp'), may hold values from -14 to 0
- w_out: bfloat16 [1024, 2048], P(None, 'tp'), may hold values from -0.75 to 0.75
- expert_rows: bfloat16 [4096, 2048], P('ep'), may hold values from -6 to 6
- expert_gain: float32 [2048], replicated, may hold values from 0.1 to 1.9
- routes: int32 [4096, 4], P('ep'), may hold values from 0 to 31, all different within a row; in each aligned block of 128 rows (0 to 127, 128 to 255, ...) at most 32 rows name the same one
- route_weight: float32 [4096, 4], P('ep'), may hold values from 0.05 to 0.6
- w_gate: bfloat16 [32, 2048, 2048], P('ep', None, 'tp'), may hold values from -0.25 to 0.25
- w_up: bfloat16 [32, 2048, 2048], P('ep', None, 'tp'), may hold values from -0.25 to 0.25
- w_down: bfloat16 [32, 2048, 2048], P('ep', None, 'tp'), may hold values from -0.0625 to 0.0625
Outputs:
- mixer_out: bfloat16 [8192, 2048], P('ep', 'tp')
- expert_out: bfloat16 [4096, 2048], P('ep', 'tp')
Inputs may be any that keep to these rules, and one draw needn't show every extreme that they name: `routes`: each row names 4 different experts. In each aligned block of 128 rows no expert is named by more than 32 rows, and in every draw some block names some expert exactly 32 times.
All inputs are finite; a program needn't handle non-finite values.
Results may differ from a plain program's by a relative error of at most 0.0073.
Values may be sent and summed in bfloat16 or wider, within the bound.
A program may use at most 64 MiB of HBM per device.

v0:
```python
import jax
import jax.numpy as jnp
from jax import lax
from jax.sharding import Mesh
from jax.sharding import PartitionSpec as P

EP = ("ep_0", "ep_1")
norm_eps = 1e-06
glu_limit = 7.0
glu_alpha = 1.702


def in_order(blocks, dim):
    shape = list(blocks.shape[1:])
    shape[dim] *= blocks.shape[0]
    return jnp.moveaxis(blocks, 0, dim).reshape(shape)


def all_blocks(shard, axes, turns):
    blocks = shard[None]
    for k in turns:
        blocks = lax.all_gather(blocks, axes[k], axis=0, tiled=True)
    carried = [lax.axis_size(axes[k]) for k in reversed(turns)]
    blocks = blocks.reshape(*carried, *shard.shape)
    turned = sorted(range(len(turns)), key=lambda place: turns[len(turns) - 1 - place])
    return blocks.transpose(*turned, *range(len(turns), blocks.ndim)).reshape(-1, *shard.shape)


def whole_of(shard, axes, turns, dim):
    return in_order(all_blocks(shard, axes, turns), dim)


def copy_for_each(shard, axis):
    devices = lax.axis_size(axis)
    return lax.all_to_all(
        jnp.broadcast_to(shard[None], (devices, *shard.shape)), axis, 0, 0, tiled=True
    )


def gather_directly(shard, axis, dim):
    blocks = copy_for_each(shard, axis)
    return in_order(blocks, dim)


def rms_scale(source, scaling):
    floats = source.astype(jnp.float32)
    inverse = lax.rsqrt(jnp.mean(floats * floats, axis=-1, keepdims=True) + norm_eps)
    return (floats * inverse * scaling).astype(jnp.bfloat16)


def stick_block(queries, packed, shifting, carried, allowed):
    length, head_count, head_width = queries.shape
    key_part = packed[:, : head_count * head_width].reshape(length, head_count, head_width)
    value_part = packed[:, head_count * head_width :].reshape(length, head_count, head_width)
    scores = jnp.einsum("thd,shd->hts", queries, key_part, preferred_element_type=jnp.float32)
    scores = scores * head_width ** (-0.5) + shifting[:, None, :]
    log_stay = jnp.where(allowed, jax.nn.log_sigmoid(-scores), 0.0)
    between = lax.cumsum(log_stay, axis=2, reverse=True) - log_stay
    weights = jnp.where(
        allowed, jnp.exp(jax.nn.log_sigmoid(scores) + between + carried[:, :, None]), 0.0
    )
    contrib = jnp.einsum(
        "hts,shd->thd", weights.astype(jnp.bfloat16), value_part, preferred_element_type=jnp.float32
    )
    return (contrib, carried + jnp.sum(log_stay, axis=2))


def per_device(
    mixer_rows,
    mixer_gain,
    w_query,
    w_key,
    w_value,
    key_shift,
    w_out,
    expert_rows,
    expert_gain,
    routes,
    route_weight,
    w_gate,
    w_up,
    w_down,
):
    length = mixer_rows.shape[0]
    head_count = key_shift.shape[0]
    head_width = w_query.shape[1] // head_count
    normed = rms_scale(mixer_rows, mixer_gain)
    queries = jnp.dot(normed, w_query, preferred_element_type=jnp.float32).astype(jnp.bfloat16)
    key_rows = jnp.dot(normed, w_key, preferred_element_type=jnp.float32).astype(jnp.bfloat16)
    value_rows = jnp.dot(normed, w_value, preferred_element_type=jnp.float32).astype(jnp.bfloat16)
    queries = queries.reshape(length, head_count, head_width)
    packed = jnp.concatenate([key_rows, value_rows], axis=1)
    device = lax.axis_index(EP)
    positions = jnp.arange(length, dtype=jnp.int32)
    strict = (positions[None, :] < positions[:, None])[None]
    own_shift = lax.dynamic_slice_in_dim(key_shift, device * length, length, 1)
    summed, carried = stick_block(
        queries, packed, own_shift, jnp.zeros((head_count, length), jnp.float32), strict
    )
    gathered = whole_of(packed, EP, (0, 1), 0)

    def visiting(offset, status):
        running, carry_now = status
        anchor = device - offset
        block_rows = lax.dynamic_slice_in_dim(gathered, anchor * length, length, 0)
        shifting = lax.dynamic_slice_in_dim(key_shift, anchor * length, length, 1)
        contrib, carry_now = stick_block(queries, block_rows, shifting, carry_now, True)
        return (running + contrib, carry_now)

    summed, carried = lax.fori_loop(1, device + 1, visiting, (summed, carried))
    head_out = summed.reshape(length, head_count * head_width).astype(jnp.bfloat16)
    weight_rows = w_out
    mixer_out = jnp.dot(
        gather_directly(head_out, "tp", 1), weight_rows, preferred_element_type=jnp.float32
    ).astype(jnp.bfloat16)
    tokens_here, top_count = routes.shape
    expert_count = lax.axis_size(EP)
    capacity = 2 * tokens_here * top_count // expert_count
    rows_after_norm = rms_scale(expert_rows, expert_gain)
    chosen = routes.reshape(-1)
    hit_table = (chosen[:, None] == jnp.arange(expert_count, dtype=jnp.int32)[None, :]).astype(
        jnp.int32
    )
    places = jnp.sum((jnp.cumsum(hit_table, axis=0) - 1) * hit_table, axis=1)
    targets = chosen * capacity + places
    assign_ids = jnp.arange(tokens_here * top_count, dtype=jnp.int32) // top_count
    owners = (
        jnp.full((expert_count * capacity,), tokens_here, jnp.int32).at[targets].set(assign_ids)
    )
    padded = jnp.concatenate(
        [rows_after_norm, jnp.zeros((1, rows_after_norm.shape[1]), jnp.bfloat16)], axis=0
    )
    outgoing = padded[owners].reshape(expert_count, capacity, rows_after_norm.shape[1])
    gate_cols = w_gate[0]
    upper_cols = w_up[0]
    down_rows = w_down[0]
    portion_size = capacity // lax.axis_size("tp")
    own_slots = lax.dynamic_slice_in_dim(
        outgoing, lax.axis_index("tp") * portion_size, portion_size, 1
    )
    arrived = lax.all_to_all(own_slots, EP, split_axis=0, concat_axis=0, tiled=True)
    expert_arrived = lax.all_gather(arrived, "tp", axis=1, tiled=True)
    expert_senders, slots_here, feature_count = expert_arrived.shape
    flat_rows = expert_arrived.reshape(expert_senders * slots_here, feature_count)
    gating = jnp.minimum(
        jnp.dot(flat_rows, gate_cols, preferred_element_type=jnp.float32), glu_limit
    )
    linear = jnp.clip(
        jnp.dot(flat_rows, upper_cols, preferred_element_type=jnp.float32), -glu_limit, glu_limit
    )
    hidden = gating * jax.nn.sigmoid(glu_alpha * gating) * (linear + 1.0)
    hidden = hidden.astype(jnp.bfloat16).reshape(expert_senders, slots_here, gate_cols.shape[1])
    senders = hidden.shape[0]
    slot_total = hidden.shape[1]
    portion_units = lax.all_gather(hidden, "tp", axis=2, tiled=True)
    weight_rows = down_rows
    flat_units = portion_units.reshape(senders * slot_total, portion_units.shape[2])
    results = jnp.dot(flat_units, weight_rows, preferred_element_type=jnp.float32)
    leaving = results.astype(jnp.bfloat16).reshape(senders, slot_total, down_rows.shape[1])
    returned = lax.all_to_all(leaving, EP, split_axis=0, concat_axis=0, tiled=True)
    picked = returned.reshape(expert_count * capacity, down_rows.shape[1])[targets].astype(
        jnp.float32
    )
    picked = picked * route_weight.reshape(-1)[:, None]
    expert_out = jnp.sum(picked.reshape(tokens_here, top_count, down_rows.shape[1]), axis=1).astype(
        jnp.bfloat16
    )
    return (mixer_out, expert_out)


def solution(mesh):
    torus = Mesh(mesh.devices.reshape(16, 2, mesh.shape["tp"]), ("ep_0", "ep_1", "tp"))
    return jax.shard_map(
        per_device,
        mesh=torus,
        in_specs=(
            P(EP, None),
            P(),
            P(None, "tp"),
            P(None, "tp"),
            P(None, "tp"),
            P("tp", None),
            P(None, "tp"),
            P(EP, None),
            P(),
            P(EP, None),
            P(EP, None),
            P(EP, None, "tp"),
            P(EP, None, "tp"),
            P(EP, None, "tp"),
        ),
        out_specs=(P(EP, "tp"), P(EP, "tp")),
        check_vma=False,
    )
```

profile of v0, /device:TPU:1, one launch (start us, length us, event | category | flops | bytes accessed | tf_op | source)
XLA Modules:
  0.0 366.4 jit_solution(1222065985565656454)
XLA Ops:
  7.3 1.6 fusion.17
  8.9 1.8 convolution_convert_fusion.2
  10.8 0.5 convolution_convert_fusion.4
  11.3 0.6 pad_maximum_fusion
  12.0 0.1 copy.63
  12.3 0.2 fusion.24
  12.5 1.2 reduce-window.26
  13.6 0.2 fusion.26
  13.9 0.2 slice_reduce_fusion
  14.1 0.1 eq.25
  14.2 0.1 copy.62
  14.3 0.1 mul.115
  14.6 2.4 scatter_custom_fusion
  17.1 6.0 %gather_fusion = bf16[1024,2048]{1,0:T(8,128)(2,1)} fusion(bf16[129,2048]{1,0:T(8,128)(2,1)S(1)} %concatenate.7, s32[1024]{0:T(1024)S(1)} %fusion.44), kind=kCustom, calls=%fused_computation | custom fusion | bytes 8392704 | tf_op jit(solution)/shard_map/gather | solution.py:133
  23.1 1.5 constant_dynamic-slice_fusion.1
  24.6 40.3 %all_to_all.15 = bf16[32,2,2048]{2,1,0:T(2,128)(2,1)S(1)} all-to-all(bf16[32,2,2048]{2,1,0:T(2,128)(2,1)S(1)} %constant_dynamic-slice_fusion.1), channel_id=1, replica_groups=mesh['ep_0'=16,'ep_1'=2,'tp'=16] {'ep_0','ep_1'}, dimensions={0} | all-to-all | bytes 524288 | tf_op jit(solution)/shard_map/all_to_all | solution.py:141
  64.9 0.8 copy.66
  65.8 19.3 %all-gather.12.cloned.1.call-done = bf16[4096,128]{0,1:T(8,128)(2,1)} async-done(((bf16[256,128]{0,1:T(8,128)(2,1)}), bf16[4096,128]{0,1:T(8,128)(2,1)}) %all-gather.12.cloned.1.call-update) | async-done | bytes 1048592 | tf_op jit(solution)/shard_map/all_gather | solution.py:22
  85.1 2.5 copy.70
  87.6 0.2 all-gather.10.cloned.1.call-start
  87.8 72.1 %all-gather.8.cloned.1.call-done = bf16[32,32,2048]{2,0,1:T(8,128)(2,1)} async-done(((bf16[32,2,2048]{2,0,1:T(8,128)(2,1)}), bf16[32,32,2048]{2,0,1:T(8,128)(2,1)}) %all-gather.8.cloned.1.call-update) | async-done | bytes 4194320 | tf_op jit(solution)/shard_map/all_gather | solution.py:142
  159.9 4.5 %copy.67 = bf16[32,32,2048]{2,1,0:T(8,128)(2,1)S(1)} copy(bf16[32,32,2048]{2,0,1:T(8,128)(2,1)} %all-gather.8.cloned.1.call-done) | data formatting | bytes 8388608 | tf_op jit(solution)/shard_map/all_gather | solution.py:142
  164.4 1.3 convolution_minimum_fusion
  165.7 2.0 fusion.22
  167.7 0.7 constant_dynamic-slice_fusion.2
  168.4 0.5 convolution_convert_fusion.3
  168.9 0.4 fusion.50
  169.3 2.3 fusion.39
  171.6 0.3 fusion.34
  171.9 0.1 convolution_bitcast_fusion.1
  172.1 12.4 %all-gather.6.cloned.1.call-done = bf16[32,256,128]{1,0,2:T(8,128)(2,1)} async-done(((bf16[16,256,128]{1,0,2:T(8,128)(2,1)}), bf16[32,256,128]{1,0,2:T(8,128)(2,1)}) %all-gather.6.cloned.1.call-update) | async-done | bytes 2097168 | tf_op jit(solution)/shard_map/all_gather | solution.py:22
  184.5 3.5 copy.61
  187.9 4.1 %while.12 = (s32[]{:T(128)}, f32[256,1,64]{0,2,1:T(8,128)S(1)}, f32[1,256]{1,0:T(1,128)S(1)}, s32[]{:T(128)}, s32[]{:T(128)}, /*index=5*/bf16[8192,128]{1,0:T(8,...) while((s32[]{:T(128)}, f32[256,1,64]{0,2,1:T(8,128)S(1)}, ...), condition=%wide.region_8.9_spmd, body=%wide.region_4.8_spmd.sunk | while | flops 27083784 | bytes 2680031 | solution.py:110
  188.0 0.7 constant_dynamic-slice_fusion.4
  188.7 0.3 fusion.77
  189.0 2.3 fusion.78
  191.4 0.4 fusion.79
  191.7 0.3 fusion.80
  192.1 0.8 broadcast_in_dim.17
  192.9 5.5 %all-to-all-start = ((bf16[16,256,64]{1,2,0:T(8,128)(2,1)}), bf16[16,256,64]{1,2,0:T(8,128)(2,1)S(1)}, u32[]{:S(2)}, u32[]{:S(2)}) async-start(bf16[16,256,64]{1,2,0:T(8,128)(2,1)} %broadcast_in_dim.17), calls=%async_computation | async-start | bytes 1048576 | tf_op jit(solution)/shard_map/all_to_all | solution.py:35
  198.4 59.6 %all-gather.10.cloned.1.call-done = bf16[32,32,2048]{2,1,0:T(8,128)(2,1)} async-done(((bf16[32,32,128]{2,1,0:T(8,128)(2,1)}), bf16[32,32,2048]{2,1,0:T(8,128)(2,1)}) %all-gather.10.cloned.1.call-update) | async-done | bytes 4194320 | tf_op jit(solution)/shard_map/all_gather | solution.py:155
  258.0 4.3 %convolution_convert_fusion = bf16[1024,128]{1,0:T(8,128)(2,1)} fusion(bf16[1024,2048]{1,0:T(8,128)(2,1)} %bitcast.152, bf16[1,2048,128]{2,1,0:T(8,128)(2,1)} %param.29), kind=kOutput, calls=%fused_computation.40 | convolution fusion | flops 537001984 | bytes 4980736 | tf_op jit(solution)/shard_map/dot_general | solution.py:158
  262.3 73.1 %all-to-all-start.2 = ((bf16[32,32,128]{2,1,0:T(8,128)(2,1)}), bf16[32,32,128]{2,1,0:T(8,128)(2,1)S(1)}, u32[]{:S(2)}, u32[]{:S(2)}) async-start(bf16[32,32,128]{2,1,0:T(8,128)(2,1)} %bitcast.38), calls=%async_computation.2 | async-start | bytes 524288 | tf_op jit(solution)/shard_map/all_to_all | solution.py:160
  335.4 0.1 copy.68
  335.5 1.0 convolution_convert_fusion.1
  336.5 21.1 %all-to-all-done.2 = bf16[32,32,128]{2,1,0:T(8,128)(2,1)S(1)} async-done(((bf16[32,32,128]{2,1,0:T(8,128)(2,1)}), bf16[32,32,128]{2,1,0:T(8,128)(2,1)S(1)}, u32[]{:S(2)}, u32[]{:S(2)}) %all-to-all-start.2) | async-done | bytes 262176 | tf_op jit(solution)/shard_map/all_to_all | solution.py:160
  357.6 1.3 gather_fusion.1
  359.0 0.9 fusion.37
  (54 shorter events, 0.7 us)
Async XLA Ops:
  7.2 157.2 %copy-start = (bf16[1,2048,128]{2,1,0:T(8,128)(2,1)S(1)}, bf16[1,2048,128]{2,1,0:T(8,128)(2,1)}, u32[]{:S(2)}) copy-start(bf16[1,2048,128]{2,1,0:T(8,128)(2,1)} %param.27) | copy-start | bytes 1572868
  7.2 3.6 copy-start.2
  7.2 3.6 copy-start.10
  7.2 3.6 copy-start.8
  7.2 77.9 %all-gather.12.cloned.1.call-start = ((), (), s32[]{:S(2)}) async-start(), calls=%async_computation.6 | async-start | bytes 1114112 | tf_op jit(solution)/shard_map/all_gather | solution.py:22
  8.9 3.1 copy-start.5
  8.9 3.4 copy-start.1
  10.8 2.9 copy-start.4
  12.0 147.9 %all-gather.8.cloned.1.call-start = ((), (), s32[]{:S(2)}) async-start(), calls=%async_computation.4 | async-start | bytes 4456448 | tf_op jit(solution)/shard_map/all_gather | solution.py:142
  65.8 118.7 %all-gather.6.cloned.1.call-start = ((), (), s32[]{:S(2)}) async-start(), calls=%async_computation.3 | async-start | bytes 3145728 | tf_op jit(solution)/shard_map/all_gather | solution.py:22
  87.6 170.4 %all-gather.10.cloned.1.call-start = ((), (), s32[]{:S(2)}) async-start(), calls=%async_computation.5 | async-start | bytes 4456448 | tf_op jit(solution)/shard_map/all_gather | solution.py:155
  164.4 1.3 copy-start.7
  165.7 2.7 copy-start.9
  192.9 69.4 %all-to-all-start = ((bf16[16,256,64]{1,2,0:T(8,128)(2,1)}), bf16[16,256,64]{1,2,0:T(8,128)(2,1)S(1)}, u32[]{:S(2)}, u32[]{:S(2)}) async-start(bf16[16,256,64]{1,2,0:T(8,128)(2,1)} %broadcast_in_dim.17), calls=%async_computation | async-start | bytes 1048576 | tf_op jit(solution)/shard_map/all_to_all | solution.py:35
  258.0 77.4 %copy-start.6 = (f32[128,4]{0,1:T(4,128)S(1)}, f32[128,4]{0,1:T(4,128)}, u32[]{:S(2)}) copy-start(f32[128,4]{0,1:T(4,128)} %param.26) | copy-start | bytes 6148
  258.0 77.5 %copy-start.3 = (bf16[1024,128]{1,0:T(8,128)(2,1)S(1)}, bf16[1024,128]{1,0:T(8,128)(2,1)}, u32[]{:S(2)}) copy-start(bf16[1024,128]{1,0:T(8,128)(2,1)} %param.22) | copy-start | bytes 786436
  262.3 95.3 %all-to-all-start.2 = ((bf16[32,32,128]{2,1,0:T(8,128)(2,1)}), bf16[32,32,128]{2,1,0:T(8,128)(2,1)S(1)}, u32[]{:S(2)}, u32[]{:S(2)}) async-start(bf16[32,32,128]{2,1,0:T(8,128)(2,1)} %bitcast.38), calls=%async_computation.2 | async-start | bytes 524288 | tf_op jit(solution)/shard_map/all_to_all | solution.py:160
Sparse Core Ops, SparseCore 0:
  12.1 72.9 all-gather.11
  88.1 71.7 all-gather.7
  162.0 22.4 all-gather.5
  187.3 70.6 all-gather.9
where the time goes:
time: 367 us; the launch traced here: 366 us
  waiting for transfers between devices  185 us (50%)
  starting transfers between devices  79 us (22%)
  blocking collectives  40.3 us (11%)
  local copies, waits for them, and re-layouts  25.8 us (7%)
  between operations  14.1 us (4%)
  matrix products  12.4 us (3%)
  other arithmetic  10.2 us (3%)
    all_to_all x1, starting transfers between devices, per_device(): lax.all_to_all(leaving, EP, split_axis=0, concat_axis=0, tiled=True)  73.1 us
    all_gather x1, waiting for transfers between devices, per_device(): expert_arrived = lax.all_gather(arrived, 'tp', axis=1, tiled=True)  72.1 us
    all_gather x1, waiting for transfers between devices, per_device(): portion_units = lax.all_gather(hidden, 'tp', axis=2, tiled=True)  59.6 us
    all_to_all x1, blocking collectives, per_device(): lax.all_to_all(own_slots, EP, split_axis=0, concat_axis=0, tiled=True)  40.3 us
    all_gather x2, waiting for transfers between devices, all_blocks(): blocks = lax.all_gather(blocks, axes[k], axis=0, tiled=True)  31.7 us
    all_to_all x1, waiting for transfers between devices, per_device(): lax.all_to_all(leaving, EP, split_axis=0, concat_axis=0, tiled=True)  21.1 us
  transfers between devices with their start and end apart: 6, of which 5 were waited for; matrix products, arithmetic and copies ran while one was open for 11% of the time, Pallas kernels for 0%

commit v1 on v0

--- a/solution.py
+++ b/solution.py
@@ -3,6 +3,7 @@
 from jax import lax
 from jax.sharding import Mesh
 from jax.sharding import PartitionSpec as P
+from jax.lax import all_to_all, psum
 
 EP = ("ep_0", "ep_1")
 norm_eps = 1e-06
@@ -139,7 +140,9 @@
         outgoing, lax.axis_index("tp") * portion_size, portion_size, 1
     )
     arrived = lax.all_to_all(own_slots, EP, split_axis=0, concat_axis=0, tiled=True)
-    expert_arrived = lax.all_gather(arrived, "tp", axis=1, tiled=True)
+    expert_arrived = jnp.concatenate(
+        all_to_all(jnp.stack(psum(1, "tp") * [arrived]), "tp", 0, 0), axis=1
+    )
     expert_senders, slots_here, feature_count = expert_arrived.shape
     flat_rows = expert_arrived.reshape(expert_senders * slots_here, feature_count)
     gating = jnp.minimum(

time: 367 us -> 352 us (0.959)
  blocking collectives: 40.3 us -> 0 us
  starting transfers between devices: 79 us -> 107 us
  waiting for transfers between devices: 185 us -> 160 us
  local copies, waits for them, and re-layouts: 25.8 us -> 43.6 us
    all_gather x1 -> x0, waiting for transfers between devices: 72.1 us -> none  [per_device(): expert_arrived = lax.all_gather(arrived, 'tp', axis=1, tiled=True)]
    all_to_all x1 -> x0, blocking collectives: 40.3 us -> none  [per_device(): lax.all_to_all(own_slots, EP, split_axis=0, concat_axis=0, tiled=True)]
    all_gather x2, waiting for transfers between devices: 31.7 us -> 55.9 us  [all_blocks(): blocks = lax.all_gather(blocks, axes[k], axis=0, tiled=True)]
    all_to_all x0 -> x2, starting transfers between devices: none -> 23.7 us  [the longest x1 16.7 us: per_device(): lax.all_to_all(own_slots, EP, split_axis=0, concat_axis=0, tiled=True)]
    all_to_all x0 -> x2, waiting for transfers between devices: none -> 23.6 us  [the longest x1 22 us: per_device(): lax.all_to_all(own_slots, EP, split_axis=0, concat_axis=0, tiled=True)]
    another operation x8 -> x10, local copies, waits for them, and re-layouts: 0.28 us -> 13 us  [the longest x1 7.21 us: per_device(): expert_arrived.reshape(expert_senders * slots_here, feature_count)]
    reshape x0 -> x1, local copies, waits for them, and re-layouts: none -> 8.69 us  [per_device(): jnp.concatenate(all_to_all(jnp.stack(psum(1, 'tp') * [arrived]), 'tp', 0,...]
    all_to_all x1, starting transfers between devices: 73.1 us -> 77.9 us  [per_device(): lax.all_to_all(leaving, EP, split_axis=0, concat_axis=0, tiled=True)]
  transfers between devices with their start and end apart: 6 -> 7, of which waited for: 5 -> 5; matrix products, arithmetic and copies ran while one was open for 11% -> 13% of each run, Pallas kernels for 0% -> 0%
where the time goes in v1:
time: 352 us; the launch traced here: 350 us
  waiting for transfers between devices  160 us (45%)
  starting transfers between devices  107 us (30%)
  local copies, waits for them, and re-layouts  43.6 us (12%)
  between operations  14 us (4%)
  matrix products  13.4 us (4%)
  other arithmetic  11.6 us (3%)
    all_to_all x1, starting transfers between devices, per_device(): lax.all_to_all(leaving, EP, split_axis=0, concat_axis=0, tiled=True)  77.9 us
    all_gather x1, waiting for transfers between devices, per_device(): portion_units = lax.all_gather(hidden, 'tp', axis=2, tiled=True)  59.5 us
    all_gather x2, waiting for transfers between devices, all_blocks(): blocks = lax.all_gather(blocks, axes[k], axis=0, tiled=True)  55.9 us
    all_to_all x1, waiting for transfers between devices, per_device(): lax.all_to_all(own_slots, EP, split_axis=0, concat_axis=0, tiled=True)  22 us
    all_to_all x1, waiting for transfers between devices, per_device(): lax.all_to_all(leaving, EP, split_axis=0, concat_axis=0, tiled=True)  21.1 us
    all_to_all x1, starting transfers between devices, per_device(): lax.all_to_all(own_slots, EP, split_axis=0, concat_axis=0, tiled=True)  16.7 us
    reshape x1, local copies, waits for them, and re-layouts, per_device(): jnp.concatenate(all_to_all(jnp.stack(psum(1, 'tp') * [arrived]), 'tp', 0,...  8.69 us
    another operation x1, local copies, waits for them, and re-layouts, per_device(): expert_arrived.reshape(expert_senders * slots_here, feature_count)  7.21 us
  transfers between devices with their start and end apart: 7, of which 5 were waited for; matrix products, arithmetic and copies ran while one was open for 13% of the time, Pallas kernels for 0%

profile of v1, /device:TPU:1, one launch (start us, length us, event | category | flops | bytes accessed | tf_op | source)
XLA Modules:
  0.0 350.4 jit_solution(3256165288962291582)
XLA Ops:
  7.2 0.8 copy.40
  8.2 0.7 broadcast_multiply_fusion
  8.9 1.2 reduce-window.26
  10.1 0.2 slice_reduce_fusion
  10.7 2.4 scatter_custom_fusion
  13.2 1.2 fusion.24
  14.4 1.2 fusion.26
  15.7 6.0 %gather_fusion = bf16[1024,2048]{1,0:T(8,128)(2,1)} fusion(bf16[129,2048]{1,0:T(8,128)(2,1)S(1)} %concatenate.7, s32[1024]{0:T(1024)S(1)} %fusion.44), kind=kCustom, calls=%fused_computation | custom fusion | bytes 8392704 | tf_op jit(solution)/shard_map/gather | solution.py:134
  21.8 2.2 constant_dynamic-slice_fusion.1
  23.9 16.7 %all-to-all-start.1 = ((bf16[32,2,2048]{2,1,0:T(2,128)(2,1)}), bf16[32,2,2048]{2,1,0:T(2,128)(2,1)S(1)}, u32[]{:S(2)}, u32[]{:S(2)}) async-start(bf16[32,2,2048]{2,1,0:T(2,128)(2,1)} %constant_dynamic-slice_fusion.1), calls=%async_computation.1 | async-start | bytes 524288 | tf_op jit(solution)/shard_map/all_to_all | solution.py:142
  40.7 0.3 fusion.17
  41.0 22.0 %all-to-all-done.1 = bf16[32,2,2048]{2,1,0:T(2,128)(2,1)S(1)} async-done(((bf16[32,2,2048]{2,1,0:T(2,128)(2,1)}), bf16[32,2,2048]{2,1,0:T(2,128)(2,1)S(1)}, u32[]{:S(2)}, u32[]{:S(2)}) %all-to-all-start.1) | async-done | bytes 262176 | tf_op jit(solution)/shard_map/all_to_all | solution.py:142
  62.9 5.5 %stack.2 = bf16[16,32,2,2048]{3,2,1,0:T(2,128)(2,1)} broadcast(bf16[32,2,2048]{2,1,0:T(2,128)(2,1)S(1)} %all-to-all-done.1), dimensions={1,2,3} | broadcast | bytes 4456448 | tf_op jit(solution)/shard_map/stack | solution.py:144
  68.4 6.9 %all-to-all-start.2 = ((bf16[16,32,2,2048]{3,2,1,0:T(2,128)(2,1)}), bf16[16,32,2,2048]{3,2,1,0:T(2,128)(2,1)}, u32[]{:S(2)}, u32[]{:S(2)}) async-start(bf16[16,32,2,2048]{3,2,1,0:T(2,128)(2,1)} %stack.2), calls=%async_computation.2 | async-start | bytes 8388608 | tf_op jit(solution)/shard_map/all_to_all | solution.py:144
  75.5 0.5 convolution_convert_fusion.2
  76.0 0.3 copy-done.7
  76.3 0.5 convolution_convert_fusion.4
  76.8 0.6 pad_maximum_fusion
  77.5 55.9 %all-gather.9.cloned.1.call-done = bf16[4096,128]{0,1:T(8,128)(2,1)} async-done(((bf16[256,128]{0,1:T(8,128)(2,1)}), bf16[4096,128]{0,1:T(8,128)(2,1)}) %all-gather.9.cloned.1.call-update) | async-done | bytes 1048592 | tf_op jit(solution)/shard_map/all_gather | solution.py:23
  133.5 2.5 copy.46
  136.0 0.2 all-gather.7.cloned.1.call-start
  136.2 1.7 all-to-all-done.2
  137.9 8.7 %copy.43 = bf16[32,16,2,2048]{3,2,1,0:T(2,128)(2,1)} copy(bf16[32,16,2,2048]{3,2,0,1:T(2,128)(2,1)} %bitcast.32) | data formatting | bytes 8388608 | tf_op jit(solution)/shard_map/reshape | solution.py:143
  146.5 7.2 %reshape_reshape.7 = bf16[1024,2048]{1,0:T(8,128)(2,1)} reshape(bf16[32,16,2,2048]{3,2,1,0:T(2,128)(2,1)} %copy.43) | data formatting | bytes 8388608 | tf_op jit(solution)/shard_map/reshape;reshape | solution.py:147
  153.8 3.6 %convolution_minimum_fusion = f32[1024,128]{1,0:T(8,128)S(1)} fusion(bf16[1024,2048]{1,0:T(8,128)(2,1)} %reshape_reshape.7, bf16[1,2048,128]{2,1,0:T(8,128)(2,1)S(1)} %copy-done), kind=kOutput, calls=%fused_computation.36 | convolution fusion | flops 537001984 | bytes 5242880 | tf_op jit(solution)/shard_map/dot_general | solution.py:149
  157.4 2.0 fusion.22
  159.4 0.7 constant_dynamic-slice_fusion.2
  160.1 0.5 convolution_convert_fusion.3
  160.6 0.4 fusion.50
  161.0 2.3 fusion.39
  163.3 0.3 fusion.34
  163.6 0.1 convolution_bitcast_fusion.1
  163.8 3.5 copy.38
  167.3 4.3 %while.12 = (s32[]{:T(128)}, f32[256,1,64]{0,2,1:T(8,128)S(1)}, f32[1,256]{1,0:T(1,128)S(1)}, s32[]{:T(128)}, s32[]{:T(128)}, /*index=5*/bf16[8192,128]{1,0:T(8,...) while((s32[]{:T(128)}, f32[256,1,64]{0,2,1:T(8,128)S(1)}, ...), condition=%wide.region_8.9_spmd, body=%wide.region_4.8_spmd.sunk | while | flops 27083784 | bytes 2680031 | solution.py:111
  167.5 0.7 constant_dynamic-slice_fusion.4
  168.2 0.3 fusion.77
  168.5 2.3 fusion.78
  170.9 0.4 fusion.79
  171.3 0.3 fusion.80
  171.6 0.8 broadcast_in_dim.17
  172.4 5.3 %all-to-all-start = ((bf16[16,256,64]{1,2,0:T(8,128)(2,1)}), bf16[16,256,64]{1,2,0:T(8,128)(2,1)S(1)}, u32[]{:S(2)}, u32[]{:S(2)}) async-start(bf16[16,256,64]{1,2,0:T(8,128)(2,1)} %broadcast_in_dim.17), calls=%async_computation | async-start | bytes 1048576 | tf_op jit(solution)/shard_map/all_to_all | solution.py:36
  177.7 59.5 %all-gather.7.cloned.1.call-done = bf16[32,32,2048]{2,1,0:T(8,128)(2,1)} async-done(((bf16[32,32,128]{2,1,0:T(8,128)(2,1)}), bf16[32,32,2048]{2,1,0:T(8,128)(2,1)}) %all-gather.7.cloned.1.call-update) | async-done | bytes 4194320 | tf_op jit(solution)/shard_map/all_gather | solution.py:158
  237.2 4.3 %convolution_convert_fusion = bf16[1024,128]{1,0:T(8,128)(2,1)} fusion(bf16[1024,2048]{1,0:T(8,128)(2,1)} %bitcast.150, bf16[1,2048,128]{2,1,0:T(8,128)(2,1)} %param.29), kind=kOutput, calls=%fused_computation.40 | convolution fusion | flops 537001984 | bytes 4980736 | tf_op jit(solution)/shard_map/dot_general | solution.py:161
  241.5 77.9 %all-to-all-start.3 = ((bf16[32,32,128]{2,1,0:T(8,128)(2,1)}), bf16[32,32,128]{2,1,0:T(8,128)(2,1)S(1)}, u32[]{:S(2)}, u32[]{:S(2)}) async-start(bf16[32,32,128]{2,1,0:T(8,128)(2,1)} %bitcast.38), calls=%async_computation.3 | async-start | bytes 524288 | tf_op jit(solution)/shard_map/all_to_all | solution.py:163
  319.5 1.0 convolution_convert_fusion.1
  320.5 21.1 %all-to-all-done.3 = bf16[32,32,128]{2,1,0:T(8,128)(2,1)S(1)} async-done(((bf16[32,32,128]{2,1,0:T(8,128)(2,1)}), bf16[32,32,128]{2,1,0:T(8,128)(2,1)S(1)}, u32[]{:S(2)}, u32[]{:S(2)}) %all-to-all-start.3) | async-done | bytes 262176 | tf_op jit(solution)/shard_map/all_to_all | solution.py:163
  341.7 1.3 gather_fusion.1
  343.0 0.9 fusion.37
  (53 shorter events, 1.1 us)
Async XLA Ops:
  7.2 146.6 %copy-start = (bf16[1,2048,128]{2,1,0:T(8,128)(2,1)S(1)}, bf16[1,2048,128]{2,1,0:T(8,128)(2,1)}, u32[]{:S(2)}) copy-start(bf16[1,2048,128]{2,1,0:T(8,128)(2,1)} %param.27) | copy-start | bytes 1572868
  15.7 25.0 %copy-start.2 = (bf16[256,2048]{1,0:T(8,128)(2,1)S(1)}, bf16[256,2048]{1,0:T(8,128)(2,1)}, u32[]{:S(2)}) copy-start(bf16[256,2048]{1,0:T(8,128)(2,1)} %param.16) | copy-start | bytes 3145732
  23.9 39.0 %all-to-all-start.1 = ((bf16[32,2,2048]{2,1,0:T(2,128)(2,1)}), bf16[32,2,2048]{2,1,0:T(2,128)(2,1)S(1)}, u32[]{:S(2)}, u32[]{:S(2)}) async-start(bf16[32,2,2048]{2,1,0:T(2,128)(2,1)} %constant_dynamic-slice_fusion.1), calls=%async_computation.1 | async-start | bytes 524288 | tf_op jit(solution)/shard_map/all_to_all | solution.py:142
  68.4 7.0 %copy-start.6 = (bf16[2048,64]{0,1:T(8,128)(2,1)S(1)}, bf16[2048,64]{0,1:T(8,128)(2,1)}, u32[]{:S(2)}) copy-start(bf16[2048,64]{0,1:T(8,128)(2,1)} %param.19) | copy-start | bytes 786436
  68.4 7.0 %copy-start.9 = (f32[2048]{0:T(1024)S(1)}, f32[2048]{0:T(1024)}, u32[]{:S(2)}) copy-start(f32[2048]{0:T(1024)} %param.17) | copy-start | bytes 24580
  68.4 69.4 %all-to-all-start.2 = ((bf16[16,32,2,2048]{3,2,1,0:T(2,128)(2,1)}), bf16[16,32,2,2048]{3,2,1,0:T(2,128)(2,1)}, u32[]{:S(2)}, u32[]{:S(2)}) async-start(bf16[16,32,2,2048]{3,2,1,0:T(2,128)(2,1)} %stack.2), calls=%async_computation.2 | async-start | bytes 8388608 | tf_op jit(solution)/shard_map/all_to_all | solution.py:144
  75.4 1.0 copy-start.7
  75.4 58.1 %all-gather.9.cloned.1.call-start = ((), (), s32[]{:S(2)}) async-start(), calls=%async_computation.6 | async-start | bytes 1114112 | tf_op jit(solution)/shard_map/all_gather | solution.py:23
  77.5 86.3 %all-gather.5.cloned.1.call-start = ((), (), s32[]{:S(2)}) async-start(), calls=%async_computation.4 | async-start | bytes 3145728 | tf_op jit(solution)/shard_map/all_gather | solution.py:23
  136.0 101.2 %all-gather.7.cloned.1.call-start = ((), (), s32[]{:S(2)}) async-start(), calls=%async_computation.5 | async-start | bytes 4456448 | tf_op jit(solution)/shard_map/all_gather | solution.py:158
  153.8 3.6 %copy-start.1 = (bf16[1024,2048]{1,0:T(8,128)(2,1)S(1)}, bf16[1024,2048]{1,0:T(8,128)(2,1)}, u32[]{:S(2)}) copy-start(bf16[1024,2048]{1,0:T(8,128)(2,1)} %reshape_reshape.7) | copy-start | bytes 12582916
  153.8 3.6 %copy-start.5 = (bf16[1,2048,128]{2,1,0:T(8,128)(2,1)S(1)}, bf16[1,2048,128]{2,1,0:T(8,128)(2,1)}, u32[]{:S(2)}) copy-start(bf16[1,2048,128]{2,1,0:T(8,128)(2,1)} %param.28) | copy-start | bytes 1572868
  157.4 2.7 copy-start.8
  172.4 69.1 %all-to-all-start = ((bf16[16,256,64]{1,2,0:T(8,128)(2,1)}), bf16[16,256,64]{1,2,0:T(8,128)(2,1)S(1)}, u32[]{:S(2)}, u32[]{:S(2)}) async-start(bf16[16,256,64]{1,2,0:T(8,128)(2,1)} %broadcast_in_dim.17), calls=%async_computation | async-start | bytes 1048576 | tf_op jit(solution)/shard_map/all_to_all | solution.py:36
  237.2 82.2 %copy-start.4 = (f32[128,4]{0,1:T(4,128)S(1)}, f32[128,4]{0,1:T(4,128)}, u32[]{:S(2)}) copy-start(f32[128,4]{0,1:T(4,128)} %param.26) | copy-start | bytes 6148
  237.2 82.3 %copy-start.3 = (bf16[1024,128]{1,0:T(8,128)(2,1)S(1)}, bf16[1024,128]{1,0:T(8,128)(2,1)}, u32[]{:S(2)}) copy-start(bf16[1024,128]{1,0:T(8,128)(2,1)} %param.22) | copy-start | bytes 786436
  241.5 100.1 %all-to-all-start.3 = ((bf16[32,32,128]{2,1,0:T(8,128)(2,1)}), bf16[32,32,128]{2,1,0:T(8,128)(2,1)S(1)}, u32[]{:S(2)}, u32[]{:S(2)}) async-start(bf16[32,32,128]{2,1,0:T(8,128)(2,1)} %bitcast.38), calls=%async_computation.3 | async-start | bytes 524288 | tf_op jit(solution)/shard_map/all_to_all | solution.py:163
Sparse Core Ops, SparseCore 0:
  78.8 54.6 all-gather.8
  136.1 27.3 all-gather.4
  166.5 70.6 all-gather.6
